TPU v7x, 32 devices: a whole 2x2x4 slice. The times are simulated.
32 devices in a mesh: st: 16 (over z, y, x), tp: 2 (over core).
Axes of the slice: x: 2, y: 2, z: 4, core: 2. Of those that a mesh axis runs over, the one named last changes fastest.
Arguments:
- tokens: bfloat16 [4096, 2048], P('st'), may hold values from -6 to 6
- store: bfloat16 [64, 64, 2048], P('st'), may hold values from -6 to 6
- passage_ids: int32 [64, 4], P('st'), may hold values from 0 to 63, as said below
- w_query: bfloat16 [2048, 2048], P(None, 'tp'), may hold values from -0.125 to 0.125
- w_key: bfloat16 [2048, 512], P(None, 'tp'), may hold values from -0.125 to 0.125
- w_value: bfloat16 [2048, 512], P(None, 'tp'), may hold values from -0.125 to 0.125
- w_ret_query: bfloat16 [2048, 1024], P(None, 'tp'), may hold values from -0.125 to 0.125
- w_ret_key: bfloat16 [2048, 1024], P(None, 'tp'), may hold values from -0.125 to 0.125
- w_ret_value: bfloat16 [2048, 2048], P(None, 'tp'), may hold values from -0.125 to 0.125
- ret_rate: float32 [8], P('tp'), may hold values from 0.003 to 0.03
- ret_gain: float32 [2048], P('tp'), may hold values from 0.1 to 1.9
- gate_logit: float32 [2048], P('tp'), may hold values from -2 to 2
- out_grad: bfloat16 [4096, 2048], P('st', 'tp'), may hold values from -6 to 6
Outputs:
- grad_tokens: bfloat16 [4096, 2048], P(('st', 'tp'))
- grad_store: bfloat16 [64, 64, 2048], P(('st', 'tp'))
- grad_key_weight: float32 [2048, 512], P(None, 'tp')
Inputs may be any that keep to these rules, and one draw needn't show every extreme that they name: `passage_ids`: passage p lies on index p // 4 of st. The rows of one device name exactly 1 passage of every owner, so the 4 passages of a block differ.
All inputs are finite; a program needn't handle non-finite values.
Results may differ from a plain program's by a relative error of at most 0.012.
Values may be sent and summed in bfloat16 or wider, within the bound.
A program may use at most 192 MiB of HBM per device.

v0:
```python
import jax
import jax.numpy as jnp
from jax import lax
from jax.sharding import PartitionSpec as P

HEAD = 256
BLK = 64
KP = 4
MOST = 1
EPSILON = 1.0


def retention_grads(query_rows, key_rows, value_rows, rates, gains, cotangent):
    length = query_rows.shape[0]
    heads = rates.shape[0]
    queries = query_rows.reshape(length, heads, -1)
    keyset = key_rows.reshape(length, heads, -1)
    values = value_rows.reshape(length, heads, -1)
    positions = jnp.arange(length, dtype=jnp.float32)
    distance = positions[:, None] - positions[None, :]
    damping = jnp.where(
        distance >= 0.0, jnp.exp(-rates[:, None, None] * jnp.maximum(distance, 0.0)), 0.0
    ) * queries.shape[-1] ** (-0.5)
    raw = jnp.einsum("thd,shd->hts", queries, keyset, preferred_element_type=jnp.float32)
    weights = (raw * damping).astype(jnp.bfloat16)
    mixed = jnp.einsum("hts,she->the", weights, values, preferred_element_type=jnp.float32)
    inverse = lax.rsqrt(jnp.mean(mixed * mixed, axis=-1, keepdims=True) + EPSILON)
    scaled = cotangent.astype(jnp.float32).reshape(length, heads, -1) * gains.reshape(heads, -1)
    inner = jnp.mean(scaled * mixed, axis=-1, keepdims=True)
    grad_mixed = (inverse * scaled - inverse * inverse * inverse * mixed * inner).astype(
        jnp.bfloat16
    )
    grad_weights = (
        jnp.einsum("the,she->hts", grad_mixed, values, preferred_element_type=jnp.float32) * damping
    ).astype(jnp.bfloat16)
    grad_first = (
        jnp.einsum("hts,shd->thd", grad_weights, keyset, preferred_element_type=jnp.float32)
        .astype(jnp.bfloat16)
        .reshape(length, -1)
    )
    grad_second = (
        jnp.einsum("hts,thd->shd", grad_weights, queries, preferred_element_type=jnp.float32)
        .astype(jnp.bfloat16)
        .reshape(length, -1)
    )
    grad_third = (
        jnp.einsum("hts,the->she", weights, grad_mixed, preferred_element_type=jnp.float32)
        .astype(jnp.bfloat16)
        .reshape(length, -1)
    )
    return (grad_first, grad_second, grad_third)


def against_rows(left, weight):
    return lax.dot_general(
        left, weight, (((1,), (1,)), ((), ())), preferred_element_type=jnp.float32
    )


def across_rows(left, right):
    return lax.dot_general(
        left, right, (((0,), (0,)), ((), ())), preferred_element_type=jnp.float32
    )


def per_device(
    tokens,
    store,
    passage_ids,
    w_query,
    w_key,
    w_value,
    w_ret_query,
    w_ret_key,
    w_ret_value,
    ret_rate,
    ret_gain,
    gate_logit,
    out_grad,
):
    owners = lax.axis_size("st")
    pass_dev, plen, width = store.shape
    length = tokens.shape[0]
    kv_width = w_key.shape[1]
    kv_local = kv_width // HEAD
    group = w_query.shape[1] // HEAD // kv_local
    blocks = length // BLK
    slot_ids = passage_ids.reshape(-1)
    slot_count = slot_ids.shape[0]
    slot_owner = slot_ids // pass_dev
    slot_local = slot_ids % pass_dev
    order = jnp.arange(slot_count, dtype=jnp.int32)
    same_owner = slot_owner[:, None] == slot_owner[None, :]
    rank = jnp.sum(same_owner & (order[None, :] < order[:, None]), axis=1)
    position = slot_owner * MOST + rank
    cells = owners * MOST
    placed = jnp.arange(cells, dtype=jnp.int32)[:, None] == position[None, :]
    request = (jnp.sum(jnp.where(placed, slot_local[None, :] + 1, 0), axis=1) - 1).reshape(
        owners, MOST
    )
    incoming = lax.all_to_all(request, "st", split_axis=0, concat_axis=0, tiled=True)
    wanted = incoming.reshape(-1)
    valid = wanted >= 0
    safe = jnp.maximum(wanted, 0)
    placed_bf = placed.astype(jnp.bfloat16)
    store_rows = store.reshape(-1, width)
    nothing = jnp.zeros((), jnp.bfloat16)
    own_kv = jnp.concatenate(
        [
            jnp.dot(store_rows, w_key, preferred_element_type=jnp.float32).astype(jnp.bfloat16),
            jnp.dot(store_rows, w_value, preferred_element_type=jnp.float32).astype(jnp.bfloat16),
        ],
        axis=1,
    ).reshape(pass_dev, plen, 2 * kv_width)
    reply = jnp.where(valid[:, None, None], own_kv[safe], nothing).reshape(
        owners, MOST, plen, 2 * kv_width
    )
    arrived = lax.all_to_all(reply, "st", split_axis=0, concat_axis=0, tiled=True)
    slot_kv = (
        across_rows(placed_bf, arrived.reshape(cells, -1))
        .astype(jnp.bfloat16)
        .reshape(slot_count, plen, 2 * kv_width)
    )
    factor = HEAD ** (-0.5)
    gate = jax.nn.sigmoid(gate_logit)
    query_bf = jnp.dot(tokens, w_query, preferred_element_type=jnp.float32).astype(jnp.bfloat16)
    queries = query_bf.reshape(blocks, BLK, kv_local, group, HEAD)
    keys = slot_kv[:, :, :kv_width].reshape(blocks, KP * plen, kv_local, HEAD)
    values = slot_kv[:, :, kv_width:].reshape(blocks, KP * plen, kv_local, HEAD)
    scores = (
        jnp.einsum("btkgd,bskd->bkgts", queries, keys, preferred_element_type=jnp.float32) * factor
    )
    expo = jnp.exp(scores)
    probs = expo / jnp.sum(expo, axis=-1, keepdims=True)
    probs_bf = probs.astype(jnp.bfloat16)
    attn = jnp.einsum("bkgts,bskd->btkgd", probs_bf, values, preferred_element_type=jnp.float32)
    grad_attn = out_grad.astype(jnp.float32).reshape(
        blocks, BLK, kv_local, group, HEAD
    ) * gate.reshape(kv_local, group, HEAD)
    grad_attn_bf = grad_attn.astype(jnp.bfloat16)
    grad_probs = jnp.einsum(
        "btkgd,bskd->bkgts", grad_attn_bf, values, preferred_element_type=jnp.float32
    )
    delta = jnp.moveaxis(jnp.sum(grad_attn * attn, axis=-1), 1, 3)
    grad_scores = (probs * (grad_probs - delta[..., None]) * factor).astype(jnp.bfloat16)
    grad_query = (
        jnp.einsum("bkgts,bskd->btkgd", grad_scores, keys, preferred_element_type=jnp.float32)
        .astype(jnp.bfloat16)
        .reshape(length, -1)
    )
    grad_keys = (
        jnp.einsum("bkgts,btkgd->bskd", grad_scores, queries, preferred_element_type=jnp.float32)
        .astype(jnp.bfloat16)
        .reshape(slot_count, plen, kv_width)
    )
    grad_values = (
        jnp.einsum("bkgts,btkgd->bskd", probs_bf, grad_attn_bf, preferred_element_type=jnp.float32)
        .astype(jnp.bfloat16)
        .reshape(slot_count, plen, kv_width)
    )
    slot_grad = jnp.concatenate([grad_keys, grad_values], axis=2)
    outgoing = (
        jnp.dot(placed_bf, slot_grad.reshape(slot_count, -1), preferred_element_type=jnp.float32)
        .astype(jnp.bfloat16)
        .reshape(owners, MOST, plen, 2 * kv_width)
    )
    returned = lax.all_to_all(outgoing, "st", split_axis=0, concat_axis=0, tiled=True)
    matched = (jnp.arange(pass_dev, dtype=jnp.int32)[:, None] == wanted[None, :]).astype(
        jnp.bfloat16
    )
    passage_grad = jnp.dot(
        matched, returned.reshape(cells, -1), preferred_element_type=jnp.float32
    ).reshape(pass_dev * plen, 2 * kv_width)
    key_grad = passage_grad[:, :kv_width]
    upper = key_grad.astype(jnp.bfloat16)
    lower = (key_grad - upper.astype(jnp.float32)).astype(jnp.bfloat16)
    key_term = across_rows(store_rows, upper) + across_rows(store_rows, lower)
    grad_key_weight = lax.psum(key_term, "st")
    passage_bf = passage_grad.astype(jnp.bfloat16)
    grad_store = lax.psum_scatter(
        (
            against_rows(passage_bf[:, :kv_width], w_key)
            + against_rows(passage_bf[:, kv_width:], w_value)
        ).astype(jnp.bfloat16),
        "tp",
        scatter_dimension=0,
        tiled=True,
    ).astype(jnp.float32)
    grad_store = grad_store.astype(jnp.bfloat16).reshape(-1, plen, width)
    ret_query = jnp.dot(tokens, w_ret_query, preferred_element_type=jnp.float32).astype(
        jnp.bfloat16
    )
    ret_key = jnp.dot(tokens, w_ret_key, preferred_element_type=jnp.float32).astype(jnp.bfloat16)
    ret_value = jnp.dot(tokens, w_ret_value, preferred_element_type=jnp.float32).astype(
        jnp.bfloat16
    )
    grad_rq, grad_rk, grad_rv = retention_grads(
        ret_query, ret_key, ret_value, ret_rate, ret_gain, out_grad
    )
    total = against_rows(grad_query, w_query)
    total = total + against_rows(grad_rq, w_ret_query)
    total = total + against_rows(grad_rk, w_ret_key)
    grad_tokens = lax.psum_scatter(
        (total + against_rows(grad_rv, w_ret_value)).astype(jnp.bfloat16),
        "tp",
        scatter_dimension=0,
        tiled=True,
    )
    return (grad_tokens, grad_store, grad_key_weight)


def solution(mesh):
    return jax.shard_map(
        per_device,
        mesh=mesh,
        in_specs=(
            P("st", None),
            P("st", None, None),
            P("st", None),
            P(None, "tp"),
            P(None, "tp"),
            P(None, "tp"),
            P(None, "tp"),
            P(None, "tp"),
            P(None, "tp"),
            P("tp"),
            P("tp"),
            P("tp"),
            P("st", "tp"),
        ),
        out_specs=(P(("st", "tp"), None), P(("st", "tp"), None, None), P(None, "tp")),
        check_vma=False,
    )
```

profile of v0, /device:TPU:0, one launch (start us, length us, event | category | flops | bytes accessed | tf_op | source)
XLA Modules:
  0.0 243.0 jit_solution(17686899952723807470)
XLA Ops:
  10.0 8.3 %all-to-all-start = ((s32[16,1,1]{2,1,0:T(1,128)}), s32[16,1,1]{2,1,0:T(1,128)S(1)}, u32[]{:S(2)}, u32[]{:S(2)}) async-start(s32[16,1,1]{2,1,0:T(1,128)} %copy.79), calls=%async_computation | async-start | bytes 16384 | tf_op jit(solution)/shard_map/all_to_all | solution.py:101
  18.3 2.1 convolution_convert_fusion.10
  22.9 2.7 %all-to-all-done = s32[16,1,1]{2,1,0:T(1,128)S(1)} async-done(((s32[16,1,1]{2,1,0:T(1,128)}), s32[16,1,1]{2,1,0:T(1,128)S(1)}, u32[]{:S(2)}, u32[]{:S(2)}) %all-to-all-start) | async-done | bytes 96 | tf_op jit(solution)/shard_map/all_to_all | solution.py:101
  28.2 2.4 fusion.18
  30.6 4.3 %all-to-all-start.1 = ((bf16[16,1,64,512]{3,2,1,0:T(8,128)(2,1)}), bf16[16,1,64,512]{3,2,1,0:T(8,128)(2,1)}, u32[]{:S(2)}, u32[]{:S(2)}) async-start(bf16[16,1,64,512]{3,2,1,0:T(8,128)(2,1)} %fusion.18), calls=%async_computation.1 | async-start | bytes 2097152 | tf_op jit(solution)/shard_map/all_to_all | solution.py:118
  34.9 2.2 copy.89
  37.2 2.5 %reshape.312 = f32[4,64,4,256]{3,2,1,0:T(4,128)} reshape(bf16[256,1024]{1,0:T(8,128)(2,1)} %param.25) | data formatting | bytes 1572864 | tf_op jit(solution)/shard_map/reshape | solution.py:137
  39.7 2.5 %reshape.313 = f32[4,64,1,4,256]{4,3,1,0,2:T(4,128)} reshape(bf16[256,1024]{1,0:T(8,128)(2,1)} %param.25) | data formatting | bytes 1572864 | tf_op jit(solution)/shard_map/reshape | solution.py:137
  42.2 1.9 convolution_convert_fusion.8
  45.0 3.3 %convolution_convert_fusion.9 = bf16[256,512]{1,0:T(8,128)(2,1)} fusion(bf16[256,2048]{1,0:T(8,128)(2,1)} %param.13, bf16[2048,512]{1,0:T(8,128)(2,1)} %param.20), kind=kOutput, calls=%fused_computation.40 | convolution fusion | flops 537001984 | bytes 3407872 | tf_op jit(solution)/shard_map/dot_general | solution.py:193
  49.4 4.6 %convolution_convert_fusion.5 = bf16[256,1024]{1,0:T(8,128)(2,1)} fusion(bf16[256,2048]{1,0:T(8,128)(2,1)} %param.13, bf16[2048,1024]{1,0:T(8,128)(2,1)} %param.16), kind=kOutput, calls=%fused_computation.33 | convolution fusion | flops 1074003968 | bytes 5767168 | tf_op jit(solution)/shard_map/dot_general | solution.py:126
  54.0 2.2 reshape.310
  58.7 1.8 copy.105
  68.2 6.0 %all-to-all-start.2 = ((bf16[16,1,64,512]{3,2,1,0:T(8,128)(2,1)}), bf16[16,1,64,512]{3,2,1,0:T(8,128)(2,1)}, u32[]{:S(2)}, u32[]{:S(2)}) async-start(bf16[16,1,64,512]{3,2,1,0:T(8,128)(2,1)} %bitcast.183), calls=%async_computation.3 | async-start | bytes 2097152 | tf_op jit(solution)/shard_map/all_to_all | solution.py:167
  75.9 4.0 %convolution_convert_fusion.4 = bf16[256,1024]{1,0:T(8,128)(2,1)S(1)} fusion(bf16[256,2048]{1,0:T(8,128)(2,1)} %param.13, bf16[2048,1024]{1,0:T(8,128)(2,1)} %param.21), kind=kOutput, calls=%fused_computation.32 | convolution fusion | flops 1074003968 | bytes 5767168 | tf_op jit(solution)/shard_map/dot_general | solution.py:194
  83.6 13.5 %all-to-all-done.2 = bf16[16,1,64,512]{3,2,1,0:T(8,128)(2,1)} async-done(((bf16[16,1,64,512]{3,2,1,0:T(8,128)(2,1)}), bf16[16,1,64,512]{3,2,1,0:T(8,128)(2,1)}, u32[]{:S(2)}, u32[]{:S(2)}) %all-to-all-start.2) | async-done | bytes 1048608 | tf_op jit(solution)/shard_map/all_to_all | solution.py:167
  97.2 1.8 copy.110
  100.1 2.2 reshape.329
  103.8 1.8 fusion.1
  107.4 3.7 %fusion.49 = f32[256,2048]{1,0:T(8,128)S(1)} fusion(bf16[256,1024]{0,1:T(8,128)(2,1)S(1)} %bitcast.195, bf16[2048,1024]{1,0:T(8,128)(2,1)} %param.21), kind=kOutput, calls=%fused_computation.101 | convolution fusion | flops 1073741824 | bytes 6815744 | tf_op jit(solution)/shard_map/dot_general | solution.py:55
  114.8 1.7 fusion.2
  116.7 1.8 fusion.34
  120.0 112.7 %all-reduce.2.cloned.1.call-done = f32[2048,256]{0,1:T(8,128)} async-done(((f32[2048,256]{0,1:T(8,128)}), f32[2048,256]{0,1:T(8,128)}) %all-reduce.2.cloned.1.call-update) | async-done | bytes 2097168 | tf_op jit(solution)/shard_map/psum | solution.py:178
  232.7 2.9 %copy.96 = f32[2048,256]{1,0:T(8,128)} copy(f32[2048,256]{0,1:T(8,128)} %all-reduce.2.cloned.1.call-done) | data formatting | bytes 4194304
  (114 shorter events, 34.1 us)
Async XLA Ops:
  8.0 34.2 %copy-start = (bf16[2048,512]{1,0:T(8,128)(2,1)S(1)}, bf16[2048,512]{1,0:T(8,128)(2,1)}, u32[]{:S(2)}) copy-start(bf16[2048,512]{1,0:T(8,128)(2,1)} %param.19) | copy-start | bytes 6291460
  8.0 12.5 %copy-start.1 = (bf16[4,64,2048]{2,1,0:T(8,128)(2,1)S(1)}, bf16[4,64,2048]{2,1,0:T(8,128)(2,1)}, u32[]{:S(2)}) copy-start(bf16[4,64,2048]{2,1,0:T(8,128)(2,1)} %param.14) | copy-start | bytes 3145732
  10.0 15.6 %all-to-all-start = ((s32[16,1,1]{2,1,0:T(1,128)}), s32[16,1,1]{2,1,0:T(1,128)S(1)}, u32[]{:S(2)}, u32[]{:S(2)}) async-start(s32[16,1,1]{2,1,0:T(1,128)} %copy.79), calls=%async_computation | async-start | bytes 16384 | tf_op jit(solution)/shard_map/all_to_all | solution.py:101
  18.3 2.2 copy-start.8
  30.6 28.1 %all-to-all-start.1 = ((bf16[16,1,64,512]{3,2,1,0:T(8,128)(2,1)}), bf16[16,1,64,512]{3,2,1,0:T(8,128)(2,1)}, u32[]{:S(2)}, u32[]{:S(2)}) async-start(bf16[16,1,64,512]{3,2,1,0:T(8,128)(2,1)} %fusion.18), calls=%async_computation.1 | async-start | bytes 2097152 | tf_op jit(solution)/shard_map/all_to_all | solution.py:118
  34.9 7.3 %copy-start.26 = (f32[4]{0:T(128)S(1)}, f32[4]{0:T(128)}, u32[]{:S(2)}) copy-start(f32[4]{0:T(128)} %param.22) | copy-start | bytes 52
  34.9 7.2 %copy-start.23 = (f32[1024]{0:T(1024)S(1)}, f32[1024]{0:T(1024)}, u32[]{:S(2)}) copy-start(f32[1024]{0:T(1024)} %param.23) | copy-start | bytes 12292
  34.9 7.2 %copy-start.24 = (f32[1024]{0:T(1024)S(1)}, f32[1024]{0:T(1024)}, u32[]{:S(2)}) copy-start(f32[1024]{0:T(1024)} %param.24) | copy-start | bytes 12292
  68.2 29.0 %all-to-all-start.2 = ((bf16[16,1,64,512]{3,2,1,0:T(8,128)(2,1)}), bf16[16,1,64,512]{3,2,1,0:T(8,128)(2,1)}, u32[]{:S(2)}, u32[]{:S(2)}) async-start(bf16[16,1,64,512]{3,2,1,0:T(8,128)(2,1)} %bitcast.183), calls=%async_computation.3 | async-start | bytes 2097152 | tf_op jit(solution)/shard_map/all_to_all | solution.py:167
  74.1 158.6 %all-reduce.2.cloned.1.call-start = ((), (), s32[]{:S(2)}) async-start(), calls=%async_computation.7 | async-start | bytes 4194304 | tf_op jit(solution)/shard_map/psum | solution.py:178
  75.9 4.0 %copy-start.14 = (bf16[4,256,256]{2,1,0:T(8,128)(2,1)}, bf16[4,256,256]{2,1,0:T(8,128)(2,1)S(1)}, u32[]{:S(2)}) copy-start(bf16[4,256,256]{2,1,0:T(8,128)(2,1)S(1)} %fusion.10) | copy-start | bytes 1572868
  75.9 4.0 %copy-start.2 = (f32[256,1024]{0,1:T(8,128)S(1)}, f32[256,1024]{0,1:T(8,128)}, u32[]{:S(2)}) copy-start(f32[256,1024]{0,1:T(8,128)} %copy.89) | copy-start | bytes 3145732
  102.3 1.5 copy-start.6
  105.5 1.5 copy-start.13
  105.5 1.5 copy-start.15
  105.6 130.0 %reduce-scatter.3.cloned.1.call-start = ((), (), s32[]{:S(2)}) async-start(), calls=%async_computation.5 | async-start | bytes 1572864 | tf_op jit(solution)/shard_map/reduce_scatter | solution.py:203
  107.4 3.7 %copy-start.5 = (bf16[16,64,256]{2,1,0:T(8,128)(2,1)S(1)}, bf16[16,64,256]{2,1,0:T(8,128)(2,1)}, u32[]{:S(2)}) copy-start(bf16[16,64,256]{2,1,0:T(8,128)(2,1)} %copy-done.4) | copy-start | bytes 1572868
  107.4 3.7 %copy-start.11 = (bf16[4,4,64,256]{3,2,1,0:T(8,128)(2,1)S(1)}, bf16[4,4,64,256]{3,2,1,0:T(8,128)(2,1)}, u32[]{:S(2)}) copy-start(bf16[4,4,64,256]{3,2,1,0:T(8,128)(2,1)} %copy-done.10) | copy-start | bytes 1572868
  107.4 4.5 %copy-start.25 = (bf16[2048,1024]{1,0:T(8,128)(2,1)S(1)}, bf16[2048,1024]{1,0:T(8,128)(2,1)}, u32[]{:S(2)}) copy-start(bf16[2048,1024]{1,0:T(8,128)(2,1)} %param.16) | copy-start | bytes 12582916
  113.2 1.6 copy-start.17
  113.3 1.6 copy-start.21
  114.8 1.8 copy-start.7
  116.6 119.0 %reduce-scatter.5.cloned.1.call-start = ((), (), s32[]{:S(2)}) async-start(), calls=%async_computation.6 | async-start | bytes 1572864 | tf_op jit(solution)/shard_map/reduce_scatter | solution.py:180
  116.7 1.8 copy-start.9
  (9 other events, 9.6 us)
Sparse Core Ops, SparseCore 0:
  105.7 126.9 all-reduce.1
Sparse Core Ops, SparseCore 1:
  116.7 8.7 reduce-scatter.2
  128.1 9.5 reduce-scatter.4
where the time goes:
time: 244 us; the launch traced here: 243 us
  waiting for transfers between devices  131 us (54%)
  matrix products  40.1 us (16%)
  local copies, waits for them, and re-layouts  31.6 us (13%)
  starting transfers between devices  19 us (8%)
  between operations  16 us (7%)
  other arithmetic  5.71 us (2%)
    psum x1, waiting for transfers between devices, per_device(): grad_key_weight = lax.psum(key_term, 'st')  113 us
    all_to_all x1, waiting for transfers between devices, per_device(): lax.all_to_all(outgoing, 'st', split_axis=0, concat_axis=0, tiled=True)  13.5 us
    unnamed x61, local copies, waits for them, and re-layouts  13.2 us
    dot_general x6, matrix products, against_rows(): lax.dot_general(left, weight, (((1,), (1,)), ((), ())), preferred_element...  10.7 us
    all_to_all x1, starting transfers between devices, per_device(): lax.all_to_all(request, 'st', split_axis=0, concat_axis=0, tiled=True)  8.34 us
    all_to_all x1, starting transfers between devices, per_device(): lax.all_to_all(outgoing, 'st', split_axis=0, concat_axis=0, tiled=True)  5.96 us
    reshape x2, local copies, waits for them, and re-layouts, per_device(): out_grad.astype(jnp.float32).reshape(blocks, BLK, kv_local, group, HEAD)  4.98 us
  transfers between devices with their start and end apart: 6, of which 4 were waited for; matrix products, arithmetic and copies ran while one was open for 21% of the time, Pallas kernels for 0%

commit v1 on v0

--- a/solution.py
+++ b/solution.py
@@ -175,7 +175,8 @@
     upper = key_grad.astype(jnp.bfloat16)
     lower = (key_grad - upper.astype(jnp.float32)).astype(jnp.bfloat16)
     key_term = across_rows(store_rows, upper) + across_rows(store_rows, lower)
-    grad_key_weight = lax.psum(key_term, "st")
+    parts = lax.all_gather(key_term, "st")
+    grad_key_weight = jnp.sum(parts, axis=0)
     passage_bf = passage_grad.astype(jnp.bfloat16)
     grad_store = lax.psum_scatter(
         (

time: 244 us -> 505 us (2.07)
  waiting for transfers between devices: 131 us -> 335 us
  blocking collectives: 0 us -> 30.7 us
  local copies, waits for them, and re-layouts: 31.6 us -> 58.8 us
  other arithmetic: 5.71 us -> 14.4 us
  starting transfers between devices: 19 us -> 13 us
    all_gather x0 -> x1, waiting for transfers between devices: none -> 321 us  [per_device(): parts = lax.all_gather(key_term, 'st')]
    psum x1 -> x0, waiting for transfers between devices: 113 us -> none  [per_device(): grad_key_weight = lax.psum(key_term, 'st')]
    all_to_all x0 -> x1, blocking collectives: none -> 30.7 us  [per_device(): lax.all_to_all(outgoing, 'st', split_axis=0, concat_axis=0, tiled=True)]
    unnamed x61 -> x54, local copies, waits for them, and re-layouts: 13.2 us -> 40.3 us
    all_to_all x1 -> x0, waiting for transfers between devices: 13.5 us -> none  [per_device(): lax.all_to_all(outgoing, 'st', split_axis=0, concat_axis=0, tiled=True)]
    all_to_all x1, waiting for transfers between devices: 1.66 us -> 11.9 us  [per_device(): lax.all_to_all(reply, 'st', split_axis=0, concat_axis=0, tiled=True)]
    reduce_sum x0 -> x1, other arithmetic: none -> 9.41 us  [per_device(): grad_key_weight = jnp.sum(parts, axis=0)]
    all_to_all x1 -> x0, starting transfers between devices: 5.96 us -> none  [per_device(): lax.all_to_all(outgoing, 'st', split_axis=0, concat_axis=0, tiled=True)]
  transfers between devices with their start and end apart: 6 -> 5, of which waited for: 4 -> 3; matrix products, arithmetic and copies ran while one was open for 21% -> 17% of each run, Pallas kernels for 0% -> 0%
where the time goes in v1:
time: 505 us; the launch traced here: 504 us
  waiting for transfers between devices  335 us (66%)
  local copies, waits for them, and re-layouts  58.8 us (12%)
  matrix products  35.5 us (7%)
  blocking collectives  30.7 us (6%)
  between operations  16 us (3%)
  other arithmetic  14.4 us (3%)
  starting transfers between devices  13 us (3%)
    all_gather x1, waiting for transfers between devices, per_device(): parts = lax.all_gather(key_term, 'st')  321 us
    unnamed x54, local copies, waits for them, and re-layouts  40.3 us
    all_to_all x1, blocking collectives, per_device(): lax.all_to_all(outgoing, 'st', split_axis=0, concat_axis=0, tiled=True)  30.7 us
    all_to_all x1, waiting for transfers between devices, per_device(): lax.all_to_all(reply, 'st', split_axis=0, concat_axis=0, tiled=True)  11.9 us
  transfers between devices with their start and end apart: 5, of which 3 were waited for; matrix products, arithmetic and copies ran while one was open for 17% of the time, Pallas kernels for 0%

profile of v1, /device:TPU:0, one launch (start us, length us, event | category | flops | bytes accessed | tf_op | source)
XLA Modules:
  0.0 503.7 jit_solution(15763105106193943301)
XLA Ops:
  10.0 8.3 %all-to-all-start = ((s32[16,1,1]{2,1,0:T(1,128)}), s32[16,1,1]{2,1,0:T(1,128)S(1)}, u32[]{:S(2)}, u32[]{:S(2)}) async-start(s32[16,1,1]{2,1,0:T(1,128)} %copy.77), calls=%async_computation | async-start | bytes 16384 | tf_op jit(solution)/shard_map/all_to_all | solution.py:101
  18.3 2.1 convolution_convert_fusion.10
  22.9 2.7 all-to-all-done
  26.2 1.6 gather_fusion
  28.2 2.3 fusion.18
  30.5 4.3 all-to-all-start.1
  35.0 2.5 reshape.312
  37.5 2.5 reshape.313
  40.0 4.6 convolution_convert_fusion.5
  44.6 2.2 reshape.310
  46.8 11.9 %all-to-all-done.1 = bf16[16,1,64,512]{3,2,1,0:T(8,128)(2,1)} async-done(((bf16[16,1,64,512]{3,2,1,0:T(8,128)(2,1)}), bf16[16,1,64,512]{3,2,1,0:T(8,128)(2,1)}, u32[]{:S(2)}, u32[]{:S(2)}) %all-to-all-start.1) | async-done | bytes 1048608 | tf_op jit(solution)/shard_map/all_to_all | solution.py:118
  58.7 1.8 copy.103
  67.1 30.7 %all_to_all.16 = bf16[16,1,64,512]{3,2,1,0:T(8,128)(2,1)S(1)} all-to-all(bf16[16,1,64,512]{3,2,1,0:T(8,128)(2,1)S(1)} %bitcast.192), channel_id=1, replica_groups=mesh['st'=16,'tp'=2] {'st'}, dimensions={0} | all-to-all | bytes 2097152 | tf_op jit(solution)/shard_map/all_to_all | solution.py:167
  99.5 2.2 reshape.329
  103.2 1.8 fusion.1
  106.4 2.6 convolution_convert_fusion.8
  110.1 3.9 convolution_convert_fusion.9
  114.0 1.8 copy.100
  117.5 3.5 convolution_convert_fusion.4
  129.4 1.7 fusion.2
  134.4 320.7 %all-gather.3.cloned.1.call-done = f32[32768,256]{0,1:T(8,128)} async-done(((f32[2048,256]{0,1:T(8,128)}), f32[32768,256]{0,1:T(8,128)}) %all-gather.3.cloned.1.call-update) | async-done | bytes 33554448 | tf_op jit(solution)/shard_map/all_gather | solution.py:178
  455.1 28.8 %copy.109 = f32[32,8,16,2048]{3,2,1,0:T(8,128)S(1)} copy(f32[32,8,16,2048]{3,1,2,0:T(8,128)} %bitcast.176) | data formatting | bytes 67108864
  483.9 9.4 %bitcast_reduce_fusion = f32[2048,256]{0,1:T(8,128)} fusion(f32[32,8,16,2048]{3,2,1,0:T(8,128)S(1)} %copy.109), kind=kLoop, calls=%fused_computation.3 | loop fusion | flops 7864320 | bytes 35651584 | tf_op jit(solution)/shard_map/reduce_sum | solution.py:179
  493.3 2.9 copy.94
  (107 shorter events, 30.6 us)
Async XLA Ops:
  8.0 98.4 %copy-start = (bf16[2048,512]{1,0:T(8,128)(2,1)S(1)}, bf16[2048,512]{1,0:T(8,128)(2,1)}, u32[]{:S(2)}) copy-start(bf16[2048,512]{1,0:T(8,128)(2,1)} %param.19) | copy-start | bytes 6291460
  8.0 12.5 %copy-start.2 = (bf16[4,64,2048]{2,1,0:T(8,128)(2,1)S(1)}, bf16[4,64,2048]{2,1,0:T(8,128)(2,1)}, u32[]{:S(2)}) copy-start(bf16[4,64,2048]{2,1,0:T(8,128)(2,1)} %param.14) | copy-start | bytes 3145732
  10.0 15.6 %all-to-all-start = ((s32[16,1,1]{2,1,0:T(1,128)}), s32[16,1,1]{2,1,0:T(1,128)S(1)}, u32[]{:S(2)}, u32[]{:S(2)}) async-start(s32[16,1,1]{2,1,0:T(1,128)} %copy.77), calls=%async_computation | async-start | bytes 16384 | tf_op jit(solution)/shard_map/all_to_all | solution.py:101
  18.3 2.2 copy-start.8
  30.5 28.1 %all-to-all-start.1 = ((bf16[16,1,64,512]{3,2,1,0:T(8,128)(2,1)}), bf16[16,1,64,512]{3,2,1,0:T(8,128)(2,1)}, u32[]{:S(2)}, u32[]{:S(2)}) async-start(bf16[16,1,64,512]{3,2,1,0:T(8,128)(2,1)} %fusion.18), calls=%async_computation.1 | async-start | bytes 2097152 | tf_op jit(solution)/shard_map/all_to_all | solution.py:118
  34.9 5.1 %copy-start.17 = (f32[1024]{0:T(1024)S(1)}, f32[1024]{0:T(1024)}, u32[]{:S(2)}) copy-start(f32[1024]{0:T(1024)} %param.24) | copy-start | bytes 12292
  34.9 420.2 %all-gather.3.cloned.1.call-start = ((), (), s32[]{:S(2)}) async-start(), calls=%async_computation.7 | async-start | bytes 35651584 | tf_op jit(solution)/shard_map/all_gather | solution.py:178
  61.0 1.2 copy-start.3
  61.3 1.5 copy-start.14
  101.7 1.5 copy-start.6
  105.0 1.3 copy-start.22
  105.0 1.4 copy-start.18
  105.0 391.2 %reduce-scatter.3.cloned.1.call-start = ((), (), s32[]{:S(2)}) async-start(), calls=%async_computation.5 | async-start | bytes 1572864 | tf_op jit(solution)/shard_map/reduce_scatter | solution.py:204
  115.9 1.6 copy-start.21
  121.7 2.3 copy-start.19
  124.0 1.3 copy-start.5
  124.0 1.3 copy-start.12
  124.0 2.5 copy-start.20
  127.8 1.6 copy-start.13
  129.4 2.0 copy-start.7
  131.2 1.2 copy-start.9
  131.2 365.0 %reduce-scatter.5.cloned.1.call-start = ((), (), s32[]{:S(2)}) async-start(), calls=%async_computation.6 | async-start | bytes 1572864 | tf_op jit(solution)/shard_map/reduce_scatter | solution.py:181
  131.5 1.4 copy-start.10
  483.9 12.3 %copy-start.1 = (bf16[2048,512]{1,0:T(8,128)(2,1)S(1)}, bf16[2048,512]{1,0:T(8,128)(2,1)}, u32[]{:S(2)}) copy-start(bf16[2048,512]{1,0:T(8,128)(2,1)} %param.19) | copy-start | bytes 6291460
  (4 other events, 3.8 us)
Sparse Core Ops, SparseCore 0:
  105.2 349.9 all-gather.2
Sparse Core Ops, SparseCore 1:
  131.3 6.8 reduce-scatter.2
  140.8 9.5 reduce-scatter.4
